TPU v7x, 256 devices: a whole 4x4x8 slice. The times are simulated.
256 devices in a mesh: sp: 64 (over z, y, core), tp: 4 (over x).
Axes of the slice: x: 4, y: 4, z: 8, core: 2. Of those that a mesh axis runs over, the one named last changes fastest.
Arguments:
- memory_queries: bfloat16 [32768, 1024], P('sp', 'tp'), may hold values from -8 to 8
- memory_keys: bfloat16 [32768, 1024], P('sp', 'tp'), may hold values from -8 to 8
- memory_values: bfloat16 [32768, 1024], P('sp', 'tp'), may hold values from -6 to 6
- input_gate_logits: float32 [8, 32768], P('tp', 'sp'), may hold values from -64 to 160
- forget_gate_logits: float32 [8, 32768], P('tp', 'sp'), may hold values from -0.1 to 20
- extra_log_decay: float32 [8, 32768], P('tp', 'sp'), may hold values from -1.4 to 0
- residual: bfloat16 [32768, 2048], P(('sp', 'tp')), may hold values from -6 to 6
- cell_output_weight: bfloat16 [1024, 2048], P('tp', 'sp'), may hold values from -0.1875 to 0.1875
- expert_norm_gain: float32 [2048], replicated, may hold values from 0.1 to 1.9
- expert_gate_weight: bfloat16 [64, 2048, 3584], P('sp', None, 'tp'), may hold values from -0.125 to 0.125
- expert_up_weight: bfloat16 [64, 2048, 3584], P('sp', None, 'tp'), may hold values from -0.125 to 0.125
- expert_down_weight: bfloat16 [64, 3584, 2048], P('sp', 'tp'), may hold values from -0.09375 to 0.09375
- routed_expert_index: int32 [32768, 2], P('sp'), may hold values from 0 to 63, as said below
- routed_expert_weight: float32 [32768, 2], P(('sp', 'tp')), may hold values from 0.1 to 1
Outputs:
- layer_out: bfloat16 [32768, 2048], P(('sp', 'tp'))
Inputs may be any that keep to these rules, and one draw needn't show every extreme that they name: `routed_expert_index`: each row names 2 different experts. In each aligned block of 128 rows (the rows of one device after the cell) no expert is named more than 5 times, and one expert is named exactly 5 times in every block.
All inputs are finite; a program needn't handle non-finite values.
Results may differ from a plain program's by a relative error of at most 0.013.
Values may be sent and summed in bfloat16 or wider, within the bound.
No kernel may reach another device: no remote copies, remote signals or barrier semaphores. Data moves between devices by JAX's collectives and lax.ppermute only.
A program may use at most 128 MiB of HBM per device.

v0:
```python
import jax
import jax.numpy as jnp
from jax import lax
from jax.sharding import Mesh
from jax.sharding import PartitionSpec as P

SP = ("sp_0", "sp_1", "sp_2")
SP_TP = ("sp_0", "sp_1", "sp_2", "tp")
lowest = -1e30
epsilon = 1e-06


def neutral_like(x, identity):
    return jax.tree.map(
        lambda a, e: jnp.broadcast_to(jnp.asarray(e, a.dtype), a.shape), x, identity
    )


def collected_together(x, axis):
    leaves = jax.tree.leaves(x)
    turns = sorted(range(len(leaves)), key=lambda k: -leaves[k].size)
    width = (1, *leaves[turns[0]].shape)[-1]
    lines = [
        jnp.pad(leaves[k].reshape(-1), (0, -leaves[k].size % width)).reshape(-1, width)
        for k in turns
    ]
    both, at, found = (lax.all_gather(jnp.concatenate(lines), axis), 0, {})
    for k, line in zip(turns, lines):
        piece = both[:, at : at + len(line)].reshape(len(both), -1)
        found[k] = piece[:, : leaves[k].size].reshape(-1, *leaves[k].shape)
        at += len(line)
    numbers = iter(range(len(leaves)))
    return jax.tree.map(lambda _: found[next(numbers)], x)


def prefix_by_axis(x, axes, combine, identity):
    before = start = neutral_like(x, identity)
    running = x
    for axis in reversed(axes):
        length, place = (lax.axis_size(axis), lax.axis_index(axis))
        pieces = collected_together(running, axis)
        inside, running = (start, start)
        for k in range(length):
            passed = k < place
            running = combine(running, jax.tree.map(lambda part: part[k], pieces))
            inside = jax.tree.map(lambda new, old: jnp.where(passed, new, old), running, inside)
        before = combine(inside, before)
    return before


def from_everyone(x, axis):
    copies = jnp.broadcast_to(x, (lax.axis_size(axis), *x.shape))
    return lax.all_to_all(copies, axis, split_axis=0, concat_axis=0, tiled=True)


def laid_out(pieces, dim):
    dims = list(pieces.shape[1:])
    dims[dim] *= pieces.shape[0]
    return jnp.moveaxis(pieces, 0, dim).reshape(dims)


def gathered_copies(x, axis, dim):
    pieces = from_everyone(x, axis)
    return laid_out(pieces, dim)


def in_blocks(x, dim, length):
    before, after = (x.shape[:dim], x.shape[dim + 1 :])
    return jnp.moveaxis(x.reshape(*before, length, -1, *after), dim, 0)


def sent_and_summed(x, axis, dim):
    length = lax.axis_size(axis)
    pieces = lax.all_to_all(in_blocks(x, dim, length), axis, 0, 0, tiled=True)
    return jnp.sum(pieces.astype(jnp.float32), axis=0)


def block_pass(memory, inputs):
    state_mat, state_norm, state_max = memory
    queries, keys_blk, values_blk, gate_in, forget_log_value = inputs
    length = gate_in.shape[-1]
    running = jnp.cumsum(forget_log_value, axis=-1)
    causal = jnp.arange(length)[:, None] >= jnp.arange(length)[None, :]
    exponent = running[:, :, None] - running[:, None, :] + gate_in[:, None, :]
    exponent = jnp.where(causal[None], exponent, -jnp.inf)
    carried = running + state_max[:, None]
    row_max = jnp.maximum(carried, jnp.max(exponent, axis=-1))
    decays = jnp.exp(exponent - row_max[:, :, None])
    carry_scale = jnp.exp(carried - row_max)
    dispatch_affinity = jnp.einsum("htk,hsk->hts", queries, keys_blk) * decays
    numerator = carry_scale[:, :, None] * jnp.einsum("hvk,htk->htv", state_mat, queries)
    numerator = numerator + jnp.einsum("hts,hsv->htv", dispatch_affinity, values_blk)
    denominator = carry_scale * jnp.einsum("hk,htk->ht", state_norm, queries) + jnp.sum(
        dispatch_affinity, axis=-1
    )
    final_log = running[:, -1]
    log_prev = final_log + state_max
    log_keep = final_log[:, None] - running + gate_in
    new_max = jnp.maximum(log_prev, jnp.max(log_keep, axis=-1))
    prev_scale = jnp.exp(log_prev - new_max)
    retain = jnp.exp(log_keep - new_max[:, None])
    new_mat = prev_scale[:, None, None] * state_mat + jnp.einsum(
        "hsv,hsk->hvk", retain[:, :, None] * values_blk, keys_blk
    )
    new_norm = prev_scale[:, None] * state_norm + jnp.einsum("hs,hsk->hk", retain, keys_blk)
    return ((new_mat, new_norm, new_max), (numerator, denominator, row_max))


def join_states(earlier, later):
    early_log, early_mat, early_norm, early_max = earlier
    late_log, late_mat, late_norm, late_max = later
    joined_max = jnp.maximum(early_max + late_log, late_max)
    early_scale = jnp.exp(early_max + late_log - joined_max)
    late_scale = jnp.exp(late_max - joined_max)
    joined_mat = early_scale[:, None, None] * early_mat + late_scale[:, None, None] * late_mat
    joined_norm = early_scale[:, None] * early_norm + late_scale[:, None] * late_norm
    return (early_log + late_log, joined_mat, joined_norm, joined_max)


def matrix_memory_step(
    memory_queries,
    memory_keys,
    memory_values,
    input_gate_logits,
    forget_gate_logits,
    extra_log_decay,
):
    tokens_here, channels = memory_queries.shape
    heads_here = input_gate_logits.shape[0]
    head_dim = channels // heads_here

    def heads_first(tensor):
        return jnp.transpose(
            tensor.astype(jnp.float32).reshape(tokens_here, heads_here, head_dim), (1, 0, 2)
        )

    queries = heads_first(memory_queries) * head_dim ** (-0.5)
    forget_log_value = jax.nn.log_sigmoid(forget_gate_logits) + extra_log_decay
    block_size = min(tokens_here, 256)
    block_count = tokens_here // block_size

    def split_blocks(tensor):
        return jnp.moveaxis(
            tensor.reshape((heads_here, block_count, block_size) + tensor.shape[2:]), 1, 0
        )

    def join_blocks(tensor):
        return jnp.moveaxis(tensor, 0, 1).reshape((heads_here, tokens_here) + tensor.shape[3:])

    empty_state = (
        jnp.zeros((heads_here, head_dim, head_dim), jnp.float32),
        jnp.zeros((heads_here, head_dim), jnp.float32),
        jnp.full((heads_here,), lowest, jnp.float32),
    )
    members = (
        queries,
        heads_first(memory_keys),
        heads_first(memory_values),
        input_gate_logits,
        forget_log_value,
    )
    end_state, pieces = lax.scan(
        block_pass, empty_state, tuple((split_blocks(member) for member in members))
    )
    numerator, denominator, row_max = (join_blocks(member) for member in pieces)
    running = jnp.cumsum(forget_log_value, axis=-1)
    identity = (jnp.zeros((heads_here,), jnp.float32),) + empty_state
    incoming = prefix_by_axis((running[:, -1],) + tuple(end_state), SP, join_states, identity)
    prior_mat, prior_norm, prior_max = incoming[1:]
    reached = running + prior_max[:, None]
    joined = jnp.maximum(row_max, reached)
    local_scale = jnp.exp(row_max - joined)
    carry_scale = jnp.exp(reached - joined)
    numerator = local_scale[:, :, None] * numerator + carry_scale[:, :, None] * jnp.einsum(
        "hvk,htk->htv", prior_mat, queries
    )
    denominator = local_scale * denominator + carry_scale * jnp.einsum(
        "hk,htk->ht", prior_norm, queries
    )
    guarded = jnp.maximum(jnp.abs(denominator), jnp.exp(-joined))
    return ((numerator / guarded[:, :, None]).astype(jnp.bfloat16), heads_here, head_dim)


def slot_index(ids, experts, capacity):
    flat_ids = ids.reshape(-1)
    matches = (flat_ids[:, None] == jnp.arange(experts, dtype=jnp.int32)[None, :]).astype(jnp.int32)
    before = jnp.cumsum(matches, axis=0) - matches
    return flat_ids * capacity + jnp.sum(before * matches, axis=1)


def local(
    memory_queries,
    memory_keys,
    memory_values,
    input_gate_logits,
    forget_gate_logits,
    extra_log_decay,
    residual,
    cell_output_weight,
    expert_norm_gain,
    expert_gate_weight,
    expert_up_weight,
    expert_down_weight,
    routed_expert_index,
    routed_expert_weight,
):
    hidden, heads_here, head_dim = matrix_memory_step(
        memory_queries,
        memory_keys,
        memory_values,
        input_gate_logits,
        forget_gate_logits,
        extra_log_decay,
    )
    weight_piece = gathered_copies(cell_output_weight, SP, 1)
    shaped = weight_piece.reshape(heads_here, head_dim, weight_piece.shape[1])
    partial_rows = jnp.einsum(
        "htd,hdc->tc", hidden, shaped, preferred_element_type=jnp.float32
    ).astype(jnp.bfloat16)
    projected = sent_and_summed(partial_rows.astype(jnp.float32).astype(jnp.bfloat16), "tp", 0)
    mixed_rows = (residual.astype(jnp.float32) + projected).astype(jnp.bfloat16)
    mixed_wide = mixed_rows.astype(jnp.float32)
    norm_scale = lax.rsqrt(jnp.mean(mixed_wide * mixed_wide, axis=-1, keepdims=True) + epsilon)
    normed = (mixed_wide * norm_scale * expert_norm_gain).astype(jnp.bfloat16)
    sp_size = lax.axis_size(SP)
    row_count, model_width = residual.shape
    top_count = routed_expert_index.shape[1]
    experts = sp_size * expert_gate_weight.shape[0]
    assigned = row_count * top_count
    capacity = max(2, assigned * 5 // (4 * experts))
    own_ids = lax.dynamic_slice_in_dim(
        routed_expert_index, lax.axis_index("tp") * row_count, row_count, 0
    )
    own_slots = slot_index(own_ids, experts, capacity)
    zero_row = jnp.zeros((1, model_width), jnp.bfloat16)
    padded = jnp.concatenate([normed, zero_row], axis=0)
    slot_table = jnp.full((experts * capacity,), row_count, jnp.int32)
    slot_table = slot_table.at[own_slots].set(jnp.arange(assigned, dtype=jnp.int32) // top_count)
    arrived = lax.all_gather(
        lax.all_to_all(
            padded[slot_table.reshape(experts, 1, capacity)],
            SP,
            split_axis=0,
            concat_axis=0,
            tiled=True,
        ),
        "tp",
        axis=1,
        tiled=True,
    )
    sources, owners, slot_span, width_in = arrived.shape
    flat_rows = arrived.reshape(-1, width_in)
    gate_pre = jnp.dot(flat_rows, expert_gate_weight[0], preferred_element_type=jnp.float32)
    up_pre = jnp.dot(flat_rows, expert_up_weight[0], preferred_element_type=jnp.float32)
    hidden_act = (jax.nn.silu(gate_pre) * up_pre).astype(jnp.bfloat16)
    group_term = jnp.dot(hidden_act, expert_down_weight[0], preferred_element_type=jnp.float32)
    group_term = lax.optimization_barrier(group_term.astype(jnp.bfloat16)).astype(jnp.float32)
    summed = lax.psum_scatter(
        group_term.reshape(sources, owners, slot_span, width_in).astype(jnp.bfloat16),
        "tp",
        scatter_dimension=1,
        tiled=True,
    )
    returned = lax.all_to_all(summed, SP, split_axis=0, concat_axis=0, tiled=True)
    picked = returned.reshape(experts * capacity, model_width)[own_slots]
    picked = picked.reshape(row_count, top_count, model_width).astype(jnp.float32)
    routed_sum = jnp.sum(picked * routed_expert_weight[:, :, None], axis=1)
    return (mixed_wide + routed_sum).astype(jnp.bfloat16)


def solution(mesh):
    finer = Mesh(mesh.devices.reshape(8, 4, 2, mesh.shape["tp"]), ("sp_0", "sp_1", "sp_2", "tp"))
    placed = (
        P(SP, "tp"),
        P(SP, "tp"),
        P(SP, "tp"),
        P("tp", SP),
        P("tp", SP),
        P("tp", SP),
        P(SP_TP, None),
        P("tp", SP),
        P(),
        P(SP, None, "tp"),
        P(SP, None, "tp"),
        P(SP, "tp", None),
        P(SP, None),
        P(SP_TP, None),
    )
    return jax.shard_map(
        local, mesh=finer, in_specs=placed, out_specs=P(SP_TP, None), check_vma=False
    )
```

profile of v0, /device:TPU:8, one launch (start us, length us, event | category | flops | bytes accessed | tf_op | source)
XLA Modules:
  0.0 450.7 jit_solution(14113384938206479818)
XLA Ops:
  6.6 1.1 copy.110
  8.0 1.1 copy.106
  9.8 7.3 %while.21 = (s32[]{:T(128)}, f32[2,128,128]{2,1,0:T(8,128)S(1)}, f32[2,128]{1,0:T(2,128)S(1)}, f32[2]{0:T(128)S(1)}, f32[2,2,256,128]{3,2,0,1:T(8,128)S(1)}, /*i...) while((s32[]{:T(128)}, f32[2,128,128]{2,1,0:T(8,128)S(1)}, ...), condition=%wide.region_6.7_spmd.clone, body=%wide.region_0.6_spmd.clone.sunk | while | flops 102833424 | bytes 3183522 | solution.py:162
  9.8 0.6 reduce-window.38
  13.0 0.4 convolution_add_fusion.3
  13.5 0.6 reduce-window.38
  16.7 0.4 convolution_add_fusion.3
  17.1 0.6 reduce-window.22
  18.3 2.0 all-gather.3
  20.7 13.0 %all-gather.4 = f32[4,260,128]{2,1,0:T(8,128)S(1)} all-gather(f32[1,260,128]{2,1,0:T(8,128)S(1)} %maximum_bitcast_fusion.1), channel_id=3, replica_groups=mesh['sp_0'=8,'sp_1'=4,'sp_2'=2,'tp'=4] {'sp_1'}, dimensions={0}, use_global_device_ids=true | all-gather | bytes 665600 | tf_op jit(solution)/shard_map/all_gather | solution.py:27
  34.0 0.3 fusion.48
  34.3 0.7 maximum_bitcast_fusion.2
  35.0 1.2 broadcast_in_dim.50
  36.2 12.4 %all-to-all-start = ((bf16[64,256,32]{1,2,0:T(8,128)(2,1)}), bf16[64,256,32]{1,2,0:T(8,128)(2,1)S(1)}, u32[]{:S(2)}, u32[]{:S(2)}) async-start(bf16[64,256,32]{1,2,0:T(8,128)(2,1)} %broadcast_in_dim.50), calls=%async_computation | async-start | bytes 2097152 | tf_op jit(solution)/shard_map/all_to_all | solution.py:53
  48.6 0.7 fusion.353
  49.3 0.8 fusion.351
  50.1 36.4 %all-gather.11.cloned.1.call-done = f32[8,260,128]{2,1,0:T(8,128)} async-done(((f32[1,260,128]{2,1,0:T(8,128)}), f32[8,260,128]{2,1,0:T(8,128)}) %all-gather.11.cloned.1.call-update) | async-done | bytes 1064976 | tf_op jit(solution)/shard_map/all_gather | solution.py:27
  86.5 0.8 fusion.350
  87.5 0.9 fusion.291
  88.9 2.1 fusion.349
  91.3 4.1 bitcast_convert_fusion
  95.3 4.4 all-to-all-start.1
  99.8 0.7 broadcast_multiply_fusion
  100.9 0.6 reduce-window.26
  102.1 1.4 scatter_custom_fusion
  103.8 21.2 %all-to-all-done.1 = bf16[4,128,2048]{2,1,0:T(8,128)(2,1)S(1)} async-done(((bf16[4,128,2048]{2,1,0:T(8,128)(2,1)}), bf16[4,128,2048]{2,1,0:T(8,128)(2,1)S(1)}, u32[]{:S(2)}, u32[]{:S(2)}) %all-to-all-start.1) | async-done | bytes 2097184 | tf_op jit(solution)/shard_map/all_to_all | solution.py:74
  125.1 0.4 convert_reduce_fusion
  125.9 0.6 copy-done
  126.6 2.4 gather_fusion
  129.0 0.6 reshape.2844
  129.6 60.1 %all_to_all.20 = bf16[64,1,5,2048]{3,2,1,0:T(8,128)(2,1)S(1)} all-to-all(bf16[64,1,5,2048]{3,2,1,0:T(8,128)(2,1)S(1)} %bitcast.677), channel_id=1, replica_groups=mesh['sp_0'=8,'sp_1'=4,'sp_2'=2,'tp'=4] {'sp_0','sp_1','sp_2'}, dimensions={0} | all-to-all | bytes 2621440 | tf_op jit(solution)/shard_map/all_to_all | solution.py:240
  189.7 1.9 copy.124
  191.7 53.9 %all-gather.9.cloned.1.call-done = bf16[64,4,5,2048]{3,0,2,1:T(8,128)(2,1)} async-done(((bf16[64,1,5,2048]{3,0,2,1:T(8,128)(2,1)}), bf16[64,4,5,2048]{3,0,2,1:T(8,128)(2,1)}) %all-gather.9.cloned.1.call-update) | async-done | bytes 5242896 | tf_op jit(solution)/shard_map/all_gather | solution.py:239
  245.6 8.9 %copy.125 = bf16[64,4,5,2048]{3,2,1,0:T(8,128)(2,1)} copy(bf16[64,4,5,2048]{3,0,2,1:T(8,128)(2,1)} %all-gather.9.cloned.1.call-done) | data formatting | bytes 10485760 | tf_op jit(solution)/shard_map/all_gather | solution.py:239
  254.4 10.0 %reshape.2836 = bf16[1280,2048]{1,0:T(8,128)(2,1)} reshape(bf16[64,4,5,2048]{3,2,1,0:T(8,128)(2,1)} %copy.125) | data formatting | bytes 10485760 | tf_op jit(solution)/shard_map/reshape | solution.py:252
  264.5 9.9 %fusion.36 = f32[1280,896]{1,0:T(8,128)} fusion(bf16[1280,2048]{1,0:T(8,128)(2,1)} %reshape.2836, bf16[1,2048,896]{2,1,0:T(8,128)(2,1)} %param.25), kind=kOutput, calls=%fused_computation.67 | convolution fusion | flops 4697620480 | bytes 13500416 | tf_op jit(solution)/shard_map/dot_general | solution.py:253
  274.4 17.5 %convolution_convert_fusion = bf16[1280,2048]{1,0:T(8,128)(2,1)} fusion(bf16[1,896,2048]{2,1,0:T(8,128)(2,1)} %param.27, f32[1280,896]{1,0:T(8,128)} %fusion.36, bf16[1280,2048]{1,0:T(8,128)(2,1)} %reshape.2836, bf16[1,2048,896]{2,1,0:T(8,128)(2,1)} %param.26), kind=kOutput, calls=%fused_computation.61 | convolution fusion | flops 9404743680 | bytes 22413312 | tf_op jit(solution)/shard_map/dot_general | solution.py:256
  291.9 9.8 %convert_element_type.74 = bf16[64,4,5,2048]{3,2,1,0:T(8,128)(2,1)} reshape(bf16[1280,2048]{1,0:T(8,128)(2,1)} %convolution_convert_fusion) | data formatting | bytes 10485760 | tf_op jit(solution)/shard_map/convert_element_type | solution.py:259
  301.6 9.2 %copy.126 = bf16[64,4,5,2048]{3,0,2,1:T(8,128)(2,1)} copy(bf16[64,4,5,2048]{3,2,1,0:T(8,128)(2,1)} %convert_element_type.74) | data formatting | bytes 10485760 | tf_op jit(solution)/shard_map/convert_element_type | solution.py:259
  310.9 58.6 %reduce-scatter.2.cloned.1.call-done = bf16[64,1,5,2048]{3,0,2,1:T(8,128)(2,1)} async-done(((bf16[64,4,5,2048]{3,0,2,1:T(8,128)(2,1)}), bf16[64,1,5,2048]{3,0,2,1:T(8,128)(2,1)}) %reduce-scatter.2.cloned.1.call-update) | async-done | bytes 1310736 | tf_op jit(solution)/shard_map/reduce_scatter | solution.py:258
  369.5 3.4 copy.127
  372.9 10.6 %all-to-all-start.3 = ((bf16[64,1,5,2048]{3,2,1,0:T(8,128)(2,1)}), bf16[64,1,5,2048]{3,2,1,0:T(8,128)(2,1)S(1)}, u32[]{:S(2)}, u32[]{:S(2)}) async-start(bf16[64,1,5,2048]{3,2,1,0:T(8,128)(2,1)} %copy.127), calls=%async_computation.4 | async-start | bytes 4194304 | tf_op jit(solution)/shard_map/all_to_all | solution.py:264
  383.6 51.1 %all-to-all-done.3 = bf16[64,1,5,2048]{3,2,1,0:T(8,128)(2,1)S(1)} async-done(((bf16[64,1,5,2048]{3,2,1,0:T(8,128)(2,1)}), bf16[64,1,5,2048]{3,2,1,0:T(8,128)(2,1)S(1)}, u32[]{:S(2)}, u32[]{:S(2)}) %all-to-all-start.3) | async-done | bytes 1310752 | tf_op jit(solution)/shard_map/all_to_all | solution.py:264
  434.7 0.6 reshape.2837
  435.3 2.3 gather_fusion.1
  437.6 2.4 reshape.2838
  440.1 3.2 multiply_reduce_fusion
  443.2 0.9 fusion.44
  (154 shorter events, 10.0 us)
Async XLA Ops:
  6.5 2.8 copy-start.3
  6.5 3.1 copy-start.8
  6.5 3.1 copy-start.7
  6.5 3.2 copy-start.4
  6.5 80.0 %all-gather.11.cloned.1.call-start = ((), (), s32[]{:S(2)}) async-start(), calls=%async_computation.7 | async-start | bytes 1216512 | tf_op jit(solution)/shard_map/all_gather | solution.py:27
  9.7 25.2 %copy-start.5 = (bf16[256,32]{0,1:T(8,128)(2,1)S(1)}, bf16[256,32]{0,1:T(8,128)(2,1)}, u32[]{:S(2)}) copy-start(bf16[256,32]{0,1:T(8,128)(2,1)} %param.23) | copy-start | bytes 49156
  20.4 13.4 %copy-start.12 = (f32[2]{0:T(128)}, f32[2]{0:T(128)S(1)}, u32[]{:S(2)}) copy-start(f32[2]{0:T(128)S(1)} %fusion.337) | copy-start | bytes 28
  33.8 2.3 copy-start.9
  33.8 2.3 copy-start.10
  33.8 53.6 %copy-start.13 = (f32[2]{0:T(128)}, f32[2]{0:T(128)S(1)}, u32[]{:S(2)}) copy-start(f32[2]{0:T(128)S(1)} %fusion.333) | copy-start | bytes 28
  36.2 54.8 %all-to-all-start = ((bf16[64,256,32]{1,2,0:T(8,128)(2,1)}), bf16[64,256,32]{1,2,0:T(8,128)(2,1)S(1)}, u32[]{:S(2)}, u32[]{:S(2)}) async-start(bf16[64,256,32]{1,2,0:T(8,128)(2,1)} %broadcast_in_dim.50), calls=%async_computation | async-start | bytes 2097152 | tf_op jit(solution)/shard_map/all_to_all | solution.py:53
  88.4 2.8 copy-start.14
  95.3 30.1 %copy-start.2 = (bf16[128,2048]{1,0:T(8,128)(2,1)S(1)}, bf16[128,2048]{1,0:T(8,128)(2,1)}, u32[]{:S(2)}) copy-start(bf16[128,2048]{1,0:T(8,128)(2,1)} %param.22) | copy-start | bytes 1572868
  95.3 29.7 %all-to-all-start.1 = ((bf16[4,128,2048]{2,1,0:T(8,128)(2,1)}), bf16[4,128,2048]{2,1,0:T(8,128)(2,1)S(1)}, u32[]{:S(2)}, u32[]{:S(2)}) async-start(bf16[4,128,2048]{2,1,0:T(8,128)(2,1)} %bitcast.682), calls=%async_computation.1 | async-start | bytes 4194304 | tf_op jit(solution)/shard_map/all_to_all | solution.py:74
  99.8 26.0 %copy-start.6 = (f32[2048]{0:T(1024)S(1)}, f32[2048]{0:T(1024)}, u32[]{:S(2)}) copy-start(f32[2048]{0:T(1024)} %param.24) | copy-start | bytes 24580
  99.8 145.8 %all-gather.9.cloned.1.call-start = ((), (), s32[]{:S(2)}) async-start(), calls=%async_computation.5 | async-start | bytes 6553600 | tf_op jit(solution)/shard_map/all_gather | solution.py:239
  125.7 0.8 copy-start
  191.6 177.9 %reduce-scatter.2.cloned.1.call-start = ((), (), s32[]{:S(2)}) async-start(), calls=%async_computation.6 | async-start | bytes 6553600 | tf_op jit(solution)/shard_map/reduce_scatter | solution.py:258
  310.9 72.6 %copy-start.11 = (f32[128,2]{0,1:T(2,128)S(1)}, f32[128,2]{0,1:T(2,128)}, u32[]{:S(2)}) copy-start(f32[128,2]{0,1:T(2,128)} %param.29) | copy-start | bytes 3076
  372.9 61.8 %all-to-all-start.3 = ((bf16[64,1,5,2048]{3,2,1,0:T(8,128)(2,1)}), bf16[64,1,5,2048]{3,2,1,0:T(8,128)(2,1)S(1)}, u32[]{:S(2)}, u32[]{:S(2)}) async-start(bf16[64,1,5,2048]{3,2,1,0:T(8,128)(2,1)} %copy.127), calls=%async_computation.4 | async-start | bytes 4194304 | tf_op jit(solution)/shard_map/all_to_all | solution.py:264
  437.6 5.6 %copy-start.1 = (bf16[128,2048]{1,0:T(8,128)(2,1)S(1)}, bf16[128,2048]{1,0:T(8,128)(2,1)}, u32[]{:S(2)}) copy-start(bf16[128,2048]{1,0:T(8,128)(2,1)} %copy-done) | copy-start | bytes 1572868
Sparse Core Ops, SparseCore 0:
  35.1 51.3 all-gather.10
  191.7 53.7 all-gather.8
  311.0 58.4 reduce-scatter.1
where the time goes:
time: 452 us; the launch traced here: 451 us
  waiting for transfers between devices  221 us (49%)
  blocking collectives  75.1 us (17%)
  local copies, waits for them, and re-layouts  64.7 us (14%)
  matrix products  34.4 us (8%)
  starting transfers between devices  27.4 us (6%)
  other arithmetic  13.7 us (3%)
  between operations  13.7 us (3%)
    all_to_all x1, blocking collectives, local(): lax.all_to_all(padded[slot_table.reshape(experts, 1, capacity)], SP, spli...  60.1 us
    reduce_scatter x1, waiting for transfers between devices, local(): lax.psum_scatter(group_term.reshape(sources, owners, slot_span, width_in)...  58.6 us
    all_gather x1, waiting for transfers between devices, local(): lax.all_gather(lax.all_to_all(padded[slot_table.reshape(experts, 1, capac...  53.9 us
    all_to_all x1, waiting for transfers between devices, local(): lax.all_to_all(summed, SP, split_axis=0, concat_axis=0, tiled=True)  51.1 us
    all_gather x1, waiting for transfers between devices, collected_together(): both, at, found = (lax.all_gather(jnp.concatenate(lines), axis), 0, {})  36.4 us
    all_to_all x1, waiting for transfers between devices, sent_and_summed(): pieces = lax.all_to_all(in_blocks(x, dim, length), axis, 0, 0, tiled=True)  21.2 us
    convert_element_type x2, local copies, waits for them, and re-layouts, local(): group_term.reshape(sources, owners, slot_span, width_in)  19 us
    dot_general x1, matrix products, local(): jnp.dot(hidden_act, expert_down_weight[0], preferred_element_type=jnp.flo...  17.5 us
  transfers between devices with their start and end apart: 6, of which 5 were waited for; matrix products, arithmetic and copies ran while one was open for 2% of the time, Pallas kernels for 0%

commit v1 on v0

--- a/solution.py
+++ b/solution.py
@@ -1,3 +1,4 @@
+import functools
 import jax
 import jax.numpy as jnp
 from jax import lax
@@ -8,6 +9,41 @@
 SP_TP = ("sp_0", "sp_1", "sp_2", "tp")
 lowest = -1e30
 epsilon = 1e-06
+
+
+def convert_the_shelves(incoming_x, in_dim):
+    incoming_x = jnp.moveaxis(incoming_x, 0, in_dim)
+    side_arr = incoming_x.shape
+    v_next = incoming_x.reshape(
+        *side_arr[:in_dim], side_arr[in_dim] * side_arr[in_dim + 1], *side_arr[in_dim + 2 :]
+    )
+    return v_next
+
+
+def _do_loads(mine, row_axis, out_dim):
+    n_shards = jax.lax.axis_size(row_axis)
+    made = list(map(lambda p: (p, (p + 1) % n_shards), range(n_shards)))
+    crops = [(src_i, to_i) for to_i, src_i in made]
+    long_array, block_next = ([], [])
+    dd = 0
+    while dd < n_shards - 1:
+        if dd % 2 == 0:
+            long_array.append(
+                jax.lax.ppermute(long_array[-1] if long_array else mine, row_axis, made)
+            )
+        else:
+            block_next.append(
+                jax.lax.ppermute(block_next[-1] if block_next else mine, row_axis, crops)
+            )
+        dd = dd + 1
+    piece_next = jnp.stack([*long_array[::-1], mine, *block_next], 0)
+    u_next = jax.lax.axis_index(row_axis) - len(long_array)
+    piece_next = piece_next[(jnp.arange(n_shards) - u_next) % n_shards]
+    t1 = convert_the_shelves(piece_next, out_dim)
+    return t1
+
+
+tell_series_over_axis = functools.partial(_do_loads, row_axis="tp", out_dim=1)
 
 
 def neutral_like(x, identity):
@@ -236,17 +272,14 @@
     padded = jnp.concatenate([normed, zero_row], axis=0)
     slot_table = jnp.full((experts * capacity,), row_count, jnp.int32)
     slot_table = slot_table.at[own_slots].set(jnp.arange(assigned, dtype=jnp.int32) // top_count)
-    arrived = lax.all_gather(
+    arrived = tell_series_over_axis(
         lax.all_to_all(
             padded[slot_table.reshape(experts, 1, capacity)],
             SP,
             split_axis=0,
             concat_axis=0,
             tiled=True,
-        ),
-        "tp",
-        axis=1,
-        tiled=True,
+        )
     )
     sources, owners, slot_span, width_in = arrived.shape
     flat_rows = arrived.reshape(-1, width_in)

time: 452 us -> 489 us (1.082); the launches traced: 451 us -> 479 us
  local copies, waits for them, and re-layouts: 64.7 us -> 78 us
  blocking collectives: 75.1 us -> 84.9 us
    all_gather x1 -> x0, waiting for transfers between devices: 53.9 us -> none  [local(): lax.all_gather(lax.all_to_all(padded[slot_table.reshape(experts, 1, capac...]
    ppermute x0 -> x3, waiting for transfers between devices: none -> 53.8 us  [the longest x2 53.8 us: _do_loads(): jax.lax.ppermute(long_array[-1] if long_array else mine, row_axis, made)]
    reshape x3 -> x2, local copies, waits for them, and re-layouts: 10 us -> 0.03 us  [the longest x1 10 us: local(): flat_rows = arrived.reshape(-1, width_in)]
    another operation x6 -> x7, local copies, waits for them, and re-layouts: 0.4 us -> 10.4 us  [the longest x1 10 us: local(): flat_rows = arrived.reshape(-1, width_in)]
    all_to_all x1, blocking collectives: 60.1 us -> 69.8 us  [local(): lax.all_to_all(padded[slot_table.reshape(experts, 1, capacity)], SP, spli...]
    all_gather x1 -> x0, local copies, waits for them, and re-layouts: 8.89 us -> none  [local(): lax.all_gather(lax.all_to_all(padded[slot_table.reshape(experts, 1, capac...]
    transpose x0 -> x1, local copies, waits for them, and re-layouts: none -> 8.27 us  [convert_the_shelves(): incoming_x = jnp.moveaxis(incoming_x, 0, in_dim)]
    gather x0 -> x1, local copies, waits for them, and re-layouts: none -> 8.01 us  [_do_loads(): piece_next = piece_next[(jnp.arange(n_shards) - u_next) % n_shards]]
  transfers between devices with their start and end apart: 6 -> 8, of which waited for: 5 -> 6; matrix products, arithmetic and copies ran while one was open for 2% -> 3% of each run, Pallas kernels for 0% -> 0%
where the time goes in v1:
time: 489 us; the launch traced here: 479 us
  waiting for transfers between devices  218 us (45%)
  blocking collectives  84.9 us (17%)
  local copies, waits for them, and re-layouts  78 us (16%)
  matrix products  34.6 us (7%)
  starting transfers between devices  30.7 us (6%)
  other arithmetic  18.2 us (4%)
  between operations  14.4 us (3%)
    all_to_all x1, blocking collectives, local(): lax.all_to_all(padded[slot_table.reshape(experts, 1, capacity)], SP, spli...  69.8 us
    reduce_scatter x1, waiting for transfers between devices, local(): lax.psum_scatter(group_term.reshape(sources, owners, slot_span, width_in)...  55.6 us
    ppermute x2, waiting for transfers between devices, _do_loads(): jax.lax.ppermute(long_array[-1] if long_array else mine, row_axis, made)  53.8 us
    all_to_all x1, waiting for transfers between devices, local(): lax.all_to_all(summed, SP, split_axis=0, concat_axis=0, tiled=True)  51.1 us
    all_gather x1, waiting for transfers between devices, collected_together(): both, at, found = (lax.all_gather(jnp.concatenate(lines), axis), 0, {})  36.4 us
    all_to_all x1, waiting for transfers between devices, sent_and_summed(): pieces = lax.all_to_all(in_blocks(x, dim, length), axis, 0, 0, tiled=True)  21.3 us
    convert_element_type x2, local copies, waits for them, and re-layouts, local(): group_term.reshape(sources, owners, slot_span, width_in)  19 us
    dot_general x1, matrix products, local(): jnp.dot(hidden_act, expert_down_weight[0], preferred_element_type=jnp.flo...  17.6 us
  transfers between devices with their start and end apart: 8, of which 6 were waited for; matrix products, arithmetic and copies ran while one was open for 3% of the time, Pallas kernels for 0%

profile of v1, /device:TPU:8, one launch (start us, length us, event | category | flops | bytes accessed | tf_op | source)
XLA Modules:
  0.0 479.0 jit_solution(12249007098020033880)
XLA Ops:
  6.6 1.1 copy.114
  8.0 1.1 copy.110
  9.8 7.3 %while.21 = (s32[]{:T(128)}, f32[2,128,128]{2,1,0:T(8,128)S(1)}, f32[2,128]{1,0:T(2,128)S(1)}, f32[2]{0:T(128)S(1)}, f32[2,2,256,128]{3,2,0,1:T(8,128)S(1)}, /*i...) while((s32[]{:T(128)}, f32[2,128,128]{2,1,0:T(8,128)S(1)}, ...), condition=%wide.region_6.7_spmd.clone, body=%wide.region_0.6_spmd.clone.sunk | while | flops 102833424 | bytes 3183522 | solution.py:198
  9.8 0.6 reduce-window.38
  13.5 0.6 reduce-window.38
  17.1 0.6 reduce-window.22
  18.3 2.0 all-gather.3
  20.7 13.0 %all-gather.4 = f32[4,260,128]{2,1,0:T(8,128)S(1)} all-gather(f32[1,260,128]{2,1,0:T(8,128)S(1)} %maximum_bitcast_fusion.2), channel_id=3, replica_groups=mesh['sp_0'=8,'sp_1'=4,'sp_2'=2,'tp'=4] {'sp_1'}, dimensions={0}, use_global_device_ids=true | all-gather | bytes 665600 | tf_op jit(solution)/shard_map/all_gather | solution.py:63
  34.3 0.7 maximum_bitcast_fusion.3
  35.0 1.2 broadcast_in_dim.50
  36.2 12.4 %all-to-all-start = ((bf16[64,256,32]{1,2,0:T(8,128)(2,1)}), bf16[64,256,32]{1,2,0:T(8,128)(2,1)S(1)}, u32[]{:S(2)}, u32[]{:S(2)}) async-start(bf16[64,256,32]{1,2,0:T(8,128)(2,1)} %broadcast_in_dim.50), calls=%async_computation | async-start | bytes 2097152 | tf_op jit(solution)/shard_map/all_to_all | solution.py:89
  48.6 0.7 fusion.355
  49.3 0.8 fusion.353
  50.1 36.4 %all-gather.8.cloned.1.call-done = f32[8,260,128]{2,1,0:T(8,128)} async-done(((f32[1,260,128]{2,1,0:T(8,128)}), f32[8,260,128]{2,1,0:T(8,128)}) %all-gather.8.cloned.1.call-update) | async-done | bytes 1064976 | tf_op jit(solution)/shard_map/all_gather | solution.py:63
  86.5 0.8 fusion.352
  87.5 0.9 fusion.291
  88.8 2.1 fusion.351
  91.2 4.1 bitcast_convert_fusion
  95.3 4.4 all-to-all-start.1
  99.8 0.7 broadcast_multiply_fusion
  102.1 1.4 scatter_custom_fusion
  103.8 21.3 %all-to-all-done.1 = bf16[4,128,2048]{2,1,0:T(8,128)(2,1)S(1)} async-done(((bf16[4,128,2048]{2,1,0:T(8,128)(2,1)}), bf16[4,128,2048]{2,1,0:T(8,128)(2,1)S(1)}, u32[]{:S(2)}, u32[]{:S(2)}) %all-to-all-start.1) | async-done | bytes 2097184 | tf_op jit(solution)/shard_map/all_to_all | solution.py:110
  126.6 2.4 gather_fusion
  129.0 1.6 reshape.2889
  130.6 69.8 %all_to_all.20 = bf16[64,1,5,2048]{3,2,1,0:T(8,128)(2,1)S(1)} all-to-all(bf16[64,1,5,2048]{3,2,1,0:T(8,128)(2,1)} %bitcast.698), channel_id=1, replica_groups=mesh['sp_0'=8,'sp_1'=4,'sp_2'=2,'tp'=4] {'sp_0','sp_1','sp_2'}, dimensions={0} | all-to-all | bytes 2621440 | tf_op jit(solution)/shard_map/all_to_all | solution.py:276
  200.4 1.9 copy.128
  202.9 2.7 collective-permute-start.2
  205.6 27.2 %collective-permute-done = bf16[64,1,5,2048]{3,0,2,1:T(8,128)(2,1)S(1)} collective-permute-done((bf16[64,1,5,2048]{3,0,2,1:T(8,128)(2,1)}, bf16[64,1,5,2048]{3,0,2,1:T(8,128)(2,1)S(1)}, u32[]{:S(2)}, u32[]{:S(2)}) %collective-permute-start) | collective-permute-done | bytes 1310752 | tf_op jit(solution)/shard_map/ppermute | solution.py:32
  232.8 0.7 copy.202
  233.6 2.1 copy.201
  235.6 26.6 %collective-permute-done.1 = bf16[64,1,5,2048]{3,0,2,1:T(8,128)(2,1)} collective-permute-done((bf16[64,1,5,2048]{3,0,2,1:T(8,128)(2,1)S(1)}, bf16[64,1,5,2048]{3,0,2,1:T(8,128)(2,1)}, u32[]{:S(2)}, u32[]{:S(2)}) %collective-permute-start.1) | collective-permute-done | bytes 1310752 | tf_op jit(solution)/shard_map/ppermute | solution.py:32
  262.2 2.1 copy.203
  264.3 4.4 maximum_bitcast_fusion
  268.7 8.0 %gather_fusion.1 = bf16[4,64,5,2048]{3,2,1,0:T(8,128)(2,1)} fusion(bf16[4,64,5,2048]{3,2,1,0:T(8,128)(2,1)} %maximum_bitcast_fusion, s32[1024]{0:T(1024)S(1)} %pad_clamp_fusion.1), kind=kCustom, calls=%fused_computation.1 | custom fusion | bytes 10485776 | tf_op jit(solution)/shard_map/gather | solution.py:41
  276.7 8.3 %copy.133 = bf16[64,4,1,5,2048]{4,3,1,0,2:T(8,128)(2,1)} copy(bf16[64,4,1,5,2048]{4,3,0,1,2:T(8,128)(2,1)} %bitcast.692) | data formatting | bytes 10485760 | tf_op jit(solution)/shard_map/transpose | solution.py:15
  285.0 10.0 %reshape_reshape.10 = bf16[1280,2048]{1,0:T(8,128)(2,1)} reshape(bf16[64,4,1,5,2048]{4,3,1,0,2:T(8,128)(2,1)} %copy.133) | data formatting | bytes 10485760 | tf_op jit(solution)/shard_map/reshape;reshape | solution.py:285
  295.0 10.0 %fusion.36 = f32[1280,896]{1,0:T(8,128)} fusion(bf16[1280,2048]{1,0:T(8,128)(2,1)} %reshape_reshape.10, bf16[1,2048,896]{2,1,0:T(8,128)(2,1)} %param.25), kind=kOutput, calls=%fused_computation.69 | convolution fusion | flops 4697620480 | bytes 13500416 | tf_op jit(solution)/shard_map/dot_general | solution.py:286
  305.0 17.6 %convolution_convert_fusion = bf16[1280,2048]{1,0:T(8,128)(2,1)} fusion(bf16[1,896,2048]{2,1,0:T(8,128)(2,1)} %param.27, f32[1280,896]{1,0:T(8,128)} %fusion.36, bf16[1280,2048]{1,0:T(8,128)(2,1)} %reshape_reshape.10, bf16[1,2048,896]{2,1,0:T(8,128)(2,1)} %param.26), kind=kOutput, calls=%fused_computation.63 | convolution fusion | flops 9404743680 | bytes 22413312 | tf_op jit(solution)/shard_map/dot_general | solution.py:289
  322.6 9.8 %convert_element_type.74 = bf16[64,4,5,2048]{3,2,1,0:T(8,128)(2,1)} reshape(bf16[1280,2048]{1,0:T(8,128)(2,1)} %convolution_convert_fusion) | data formatting | bytes 10485760 | tf_op jit(solution)/shard_map/convert_element_type | solution.py:292
  332.3 9.2 %copy.134 = bf16[64,4,5,2048]{3,0,2,1:T(8,128)(2,1)} copy(bf16[64,4,5,2048]{3,2,1,0:T(8,128)(2,1)} %convert_element_type.74) | data formatting | bytes 10485760 | tf_op jit(solution)/shard_map/convert_element_type | solution.py:292
  341.6 55.6 %reduce-scatter.2.cloned.1.call-done = bf16[64,1,5,2048]{3,0,2,1:T(8,128)(2,1)} async-done(((bf16[64,4,5,2048]{3,0,2,1:T(8,128)(2,1)}), bf16[64,1,5,2048]{3,0,2,1:T(8,128)(2,1)}) %reduce-scatter.2.cloned.1.call-update) | async-done | bytes 1310736 | tf_op jit(solution)/shard_map/reduce_scatter | solution.py:291
  397.2 3.4 copy.135
  400.6 10.6 %all-to-all-start.3 = ((bf16[64,1,5,2048]{3,2,1,0:T(8,128)(2,1)}), bf16[64,1,5,2048]{3,2,1,0:T(8,128)(2,1)S(1)}, u32[]{:S(2)}, u32[]{:S(2)}) async-start(bf16[64,1,5,2048]{3,2,1,0:T(8,128)(2,1)} %copy.135), calls=%async_computation.4 | async-start | bytes 4194304 | tf_op jit(solution)/shard_map/all_to_all | solution.py:297
  411.3 51.1 %all-to-all-done.3 = bf16[64,1,5,2048]{3,2,1,0:T(8,128)(2,1)S(1)} async-done(((bf16[64,1,5,2048]{3,2,1,0:T(8,128)(2,1)}), bf16[64,1,5,2048]{3,2,1,0:T(8,128)(2,1)S(1)}, u32[]{:S(2)}, u32[]{:S(2)}) %all-to-all-start.3) | async-done | bytes 1310752 | tf_op jit(solution)/shard_map/all_to_all | solution.py:297
  462.9 2.3 gather_fusion.2
  465.3 2.4 reshape.2883
  467.7 3.2 multiply_reduce_fusion
  470.9 0.9 fusion.44
  (164 shorter events, 13.7 us)
Async XLA Ops:
  6.5 2.8 copy-start.3
  6.5 3.1 copy-start.8
  6.5 3.1 copy-start.7
  6.5 3.2 copy-start.4
  6.5 80.0 %all-gather.8.cloned.1.call-start = ((), (), s32[]{:S(2)}) async-start(), calls=%async_computation.6 | async-start | bytes 1216512 | tf_op jit(solution)/shard_map/all_gather | solution.py:63
  9.7 25.2 %copy-start.5 = (bf16[256,32]{0,1:T(8,128)(2,1)S(1)}, bf16[256,32]{0,1:T(8,128)(2,1)}, u32[]{:S(2)}) copy-start(bf16[256,32]{0,1:T(8,128)(2,1)} %param.23) | copy-start | bytes 49156
  20.4 13.4 %copy-start.12 = (f32[2]{0:T(128)}, f32[2]{0:T(128)S(1)}, u32[]{:S(2)}) copy-start(f32[2]{0:T(128)S(1)} %fusion.339) | copy-start | bytes 28
  33.8 2.3 copy-start.9
  33.8 2.3 copy-start.10
  33.8 53.5 %copy-start.13 = (f32[2]{0:T(128)}, f32[2]{0:T(128)S(1)}, u32[]{:S(2)}) copy-start(f32[2]{0:T(128)S(1)} %fusion.335) | copy-start | bytes 28
  36.2 54.8 %all-to-all-start = ((bf16[64,256,32]{1,2,0:T(8,128)(2,1)}), bf16[64,256,32]{1,2,0:T(8,128)(2,1)S(1)}, u32[]{:S(2)}, u32[]{:S(2)}) async-start(bf16[64,256,32]{1,2,0:T(8,128)(2,1)} %broadcast_in_dim.50), calls=%async_computation | async-start | bytes 2097152 | tf_op jit(solution)/shard_map/all_to_all | solution.py:89
  88.4 2.8 copy-start.14
  95.3 30.1 %copy-start.2 = (bf16[128,2048]{1,0:T(8,128)(2,1)S(1)}, bf16[128,2048]{1,0:T(8,128)(2,1)}, u32[]{:S(2)}) copy-start(bf16[128,2048]{1,0:T(8,128)(2,1)} %param.22) | copy-start | bytes 1572868
  95.3 29.7 %all-to-all-start.1 = ((bf16[4,128,2048]{2,1,0:T(8,128)(2,1)}), bf16[4,128,2048]{2,1,0:T(8,128)(2,1)S(1)}, u32[]{:S(2)}, u32[]{:S(2)}) async-start(bf16[4,128,2048]{2,1,0:T(8,128)(2,1)} %bitcast.706), calls=%async_computation.1 | async-start | bytes 4194304 | tf_op jit(solution)/shard_map/all_to_all | solution.py:110
  99.8 26.0 %copy-start.6 = (f32[2048]{0:T(1024)S(1)}, f32[2048]{0:T(1024)}, u32[]{:S(2)}) copy-start(f32[2048]{0:T(1024)} %param.24) | copy-start | bytes 24580
  99.8 297.4 %reduce-scatter.2.cloned.1.call-start = ((), (), s32[]{:S(2)}) async-start(), calls=%async_computation.5 | async-start | bytes 6553600 | tf_op jit(solution)/shard_map/reduce_scatter | solution.py:291
  125.7 0.8 copy-start
  202.4 30.4 %collective-permute-start = (bf16[64,1,5,2048]{3,0,2,1:T(8,128)(2,1)}, bf16[64,1,5,2048]{3,0,2,1:T(8,128)(2,1)S(1)}, u32[]{:S(2)}, u32[]{:S(2)}) collective-permute-start(bf16[64,1,5,2048]{3,0,2,1:T(8,128)(2,1)} %copy.128), channel_id=1, source_target_pairs={{0,1},{1,2},{2,3},{3,0},{4,5},{5,6},{6,7},{7,4},{8,9},{9,10},{10,1... | collective-permute-start | bytes 3932168 | tf_op jit(solution)/shard_map/ppermute | solution.py:32
  202.9 30.6 %collective-permute-start.2 = (bf16[64,1,5,2048]{3,0,2,1:T(8,128)(2,1)}, bf16[64,1,5,2048]{3,0,2,1:T(8,128)(2,1)}, u32[]{:S(2)}, u32[]{:S(2)}) collective-permute-start(bf16[64,1,5,2048]{3,0,2,1:T(8,128)(2,1)} %copy.128), channel_id=1, source_target_pairs={{1,0},{2,1},{3,2},{0,3},{5,4},{6,5},{7,6},{4,7},{9,8},{10,9},{11,1... | collective-permute-start | bytes 3932168 | tf_op jit(solution)/shard_map/ppermute | solution.py:36
  232.8 29.5 %collective-permute-start.1 = (bf16[64,1,5,2048]{3,0,2,1:T(8,128)(2,1)S(1)}, bf16[64,1,5,2048]{3,0,2,1:T(8,128)(2,1)}, u32[]{:S(2)}, u32[]{:S(2)}) collective-permute-start(bf16[64,1,5,2048]{3,0,2,1:T(8,128)(2,1)S(1)} %collective-permute-done), channel_id=1, source_target_pairs={{0,1},{1,2},{2,3},{3,0},{4,5},{5,6},{6,7},{7,4},{8,9},{9,10},{10,1... | collective-permute-start | bytes 3932168 | tf_op jit(solution)/shard_map/ppermute | solution.py:32
  341.6 69.6 %copy-start.11 = (f32[128,2]{0,1:T(2,128)S(1)}, f32[128,2]{0,1:T(2,128)}, u32[]{:S(2)}) copy-start(f32[128,2]{0,1:T(2,128)} %param.29) | copy-start | bytes 3076
  400.6 61.8 %all-to-all-start.3 = ((bf16[64,1,5,2048]{3,2,1,0:T(8,128)(2,1)}), bf16[64,1,5,2048]{3,2,1,0:T(8,128)(2,1)S(1)}, u32[]{:S(2)}, u32[]{:S(2)}) async-start(bf16[64,1,5,2048]{3,2,1,0:T(8,128)(2,1)} %copy.135), calls=%async_computation.4 | async-start | bytes 4194304 | tf_op jit(solution)/shard_map/all_to_all | solution.py:297
  465.3 5.6 %copy-start.1 = (bf16[128,2048]{1,0:T(8,128)(2,1)S(1)}, bf16[128,2048]{1,0:T(8,128)(2,1)}, u32[]{:S(2)}) copy-start(bf16[128,2048]{1,0:T(8,128)(2,1)} %copy-done) | copy-start | bytes 1572868
Sparse Core Ops, SparseCore 0:
  35.1 51.3 all-gather.7
  341.7 55.4 reduce-scatter.1
